TPU v7x, 128 devices: a whole 4x4x4 slice. The times are simulated.
128 devices in a mesh: kv: 16 (over z, y), tp: 8 (over x, core).
Axes of the slice: x: 4, y: 4, z: 4, core: 2. Of those that a mesh axis runs over, the one named last changes fastest.
Arguments:
- hidden_in: bfloat16 [16, 4096], P(None, ('kv', 'tp')), may hold values from -12 to 12
- attn_gain: float32 [4096], P('kv'), may hold values from 0.1 to 1.9
- query_weight: bfloat16 [4096, 4096], P('kv', 'tp'), may hold values from -0.09375 to 0.09375
- key_cache: bfloat16 [16, 16384, 8, 128], P(None, 'kv', 'tp'), may hold values from -600 to 600
- value_cache: bfloat16 [16, 16384, 8, 128], P(None, 'kv', 'tp'), may hold values from -6 to 6
- lambdas: float32 [32], P('tp'), may hold values from 0.3 to 0.8
- head_gain: float32 [128], replicated, may hold values from 0.1 to 1.9
- out_weight: bfloat16 [4096, 4096], P('tp', 'kv'), may hold values from -0.09375 to 0.09375
- mixer_gain: float32 [4096], P(('kv', 'tp')), may hold values from 0.1 to 1.9
- gate_weight: bfloat16 [4096, 11264], P('kv', 'tp'), may hold values from -0.09375 to 0.09375
- up_weight: bfloat16 [4096, 11264], P('kv', 'tp'), may hold values from -0.09375 to 0.09375
- down_weight: bfloat16 [11264, 4096], P('tp', 'kv'), may hold values from -0.0546875 to 0.0546875
Outputs:
- mixed: bfloat16 [16, 4096], P(None, ('kv', 'tp'))
All inputs are finite; a program needn't handle non-finite values.
Results may differ from a plain program's by a relative error of at most 0.017.
Values may be sent and summed in bfloat16 or wider, within the bound.
A program may use at most 64 MiB of HBM per device.

v0:
```python
import functools
import math

import jax
import jax.numpy as jnp
from jax import lax
from jax.sharding import Mesh
from jax.sharding import PartitionSpec as P

D = 4096
HEAD_DIM = 64
TP = ("tp_0", "tp_1")
KV = ("kv_0", "kv_1")
KV_TP = ("kv_0", "kv_1", "tp_0", "tp_1")


eps = 1e-06


def from_everyone(shard, axis):
    length = lax.axis_size(axis)
    return lax.all_to_all(
        jnp.broadcast_to(shard[None], (length, *shard.shape)), axis, 0, 0, tiled=True
    )


def joined_along(tiles, dim):
    shape = list(tiles.shape[1:])
    shape[dim] *= tiles.shape[0]
    return jnp.moveaxis(tiles, 0, dim).reshape(shape)


def collect(shard, axis, dim):
    tiles = from_everyone(shard, axis)
    return joined_along(tiles, dim)


def over_copies(shard, axis):
    return from_everyone(shard, axis).sum(axis=0)


def in_one(arrays, axis):
    vector, at, gathered = (jnp.concatenate([a.reshape(-1) for a in arrays]), 0, [])
    subtotal = over_copies(vector, axis)
    for a in arrays:
        gathered.append(subtotal[at : at + a.size].reshape(a.shape))
        at += a.size
    return tuple(gathered)


def side_by_side(arrays, axis, split_dim, concat_dim, along):
    widths = [math.prod(a.shape[along:]) for a in arrays]
    both = jnp.concatenate(
        [a.reshape(*a.shape[:along], w) for a, w in zip(arrays, widths)], axis=along
    )
    whole = lax.all_to_all(both, axis, split_axis=split_dim, concat_axis=concat_dim, tiled=True)
    tiles = jnp.split(whole, [sum(widths[:k]) for k in range(1, len(widths))], axis=along)
    return tuple((b.reshape(*whole.shape[:along], *a.shape[along:]) for a, b in zip(arrays, tiles)))


def cut_along(shard, dim, length):
    before, after = (shard.shape[:dim], shard.shape[dim + 1 :])
    return jnp.moveaxis(shard.reshape(*before, length, -1, *after), dim, 0)


def summed_on_arrival(shard, axis, dim):
    tiles = cut_along(shard, dim, lax.axis_size(axis))
    arrived = lax.all_to_all(tiles, axis, split_axis=0, concat_axis=0, tiled=True)
    return arrived.astype(jnp.float32).sum(axis=0)


def by_axis(shard, axes):
    return functools.reduce(lax.psum, axes, shard)


def sent_and_summed(shard, axis, dim):
    length = lax.axis_size(axis)
    tiles = lax.all_to_all(cut_along(shard, dim, length), axis, 0, 0, tiled=True)
    return jnp.sum(tiles, axis=0)


def in_one_piece(arrays, axis, dim, along):
    widths = [a.shape[along] for a in arrays]
    both = jnp.concatenate(arrays, axis=along)
    whole = sent_and_summed(both, axis, dim)
    return tuple(jnp.split(whole, [sum(widths[:k]) for k in range(1, len(widths))], axis=along))


def finish_heads(totals, weighted, lambdas, head_gain, kv_dev, group_size):
    head_means = weighted / totals[..., None]
    mixing = lambdas.reshape(kv_dev, group_size)
    attended = head_means[0] - mixing[None, :, :, None] * head_means[1]
    norm_inv = lax.rsqrt(jnp.mean(attended * attended, axis=-1, keepdims=True) + eps)
    head_out = (attended * norm_inv * head_gain).astype(jnp.bfloat16)
    return head_out.reshape(head_out.shape[0], kv_dev * group_size * 2 * HEAD_DIM)


def per_device(
    hidden_in,
    attn_gain,
    query_weight,
    key_cache,
    value_cache,
    lambdas,
    head_gain,
    out_weight,
    mixer_gain,
    gate_weight,
    up_weight,
    down_weight,
):
    batch_rows = hidden_in.shape[0]
    rows_block = collect(hidden_in, TP, 1)
    block_f = rows_block.astype(jnp.float32)
    gained = (block_f * attn_gain).astype(jnp.bfloat16)
    partial_value = jnp.dot(gained, query_weight, preferred_element_type=jnp.float32)
    query_full, squares = in_one((partial_value, jnp.sum(block_f * block_f, axis=1)), KV)
    row_scale = lax.rsqrt(squares / D + eps)
    query_rows = (query_full * row_scale[:, None]).astype(jnp.bfloat16)
    positions = key_cache.shape[1]
    kv_dev = key_cache.shape[2]
    heads_dev = query_rows.shape[1] // (2 * HEAD_DIM)
    group_size = heads_dev // kv_dev
    query_heads = query_rows.reshape(batch_rows, kv_dev, group_size, 2, HEAD_DIM)
    key_rows = key_cache.reshape(batch_rows, positions, kv_dev, 2, HEAD_DIM)
    scores = jnp.einsum(
        "bkgcd,bpkcd->cbkgp", query_heads, key_rows, preferred_element_type=jnp.float32
    ) * HEAD_DIM ** (-0.5)
    maxima = jnp.max(scores, axis=-1)
    exponent = jnp.exp(scores - maxima[..., None])
    totals = jnp.sum(exponent, axis=-1)
    exp_weights = exponent.astype(jnp.bfloat16)
    weighted = jnp.einsum(
        "cbkgp,bpkv->cbkgv", exp_weights, value_cache, preferred_element_type=jnp.float32
    )
    parts_max, parts_tot, parts_acc = side_by_side(
        (maxima[None], totals[None], weighted[None]), KV, 2, 0, 5
    )
    top = jnp.max(parts_max, axis=0)
    factors = jnp.exp(parts_max - top[None])
    own_tot = jnp.sum(parts_tot * factors, axis=0)
    own_acc = jnp.sum(parts_acc * factors[..., None], axis=0)
    own_out = finish_heads(own_tot, own_acc, lambdas, head_gain, kv_dev, group_size)
    head_out = collect(own_out, KV, 0)
    projected = jnp.dot(head_out, out_weight, preferred_element_type=jnp.float32)
    attn_out = summed_on_arrival(projected.astype(jnp.bfloat16), TP, 1)
    after_attn = (hidden_in.astype(jnp.float32) + attn_out).astype(jnp.bfloat16)
    after_f = after_attn.astype(jnp.float32)
    squares_two = by_axis(jnp.sum(after_f * after_f, axis=1), KV_TP)
    mixer_in = (after_f * lax.rsqrt(squares_two / D + eps)[:, None] * mixer_gain).astype(
        jnp.bfloat16
    )
    gathered = collect(mixer_in, TP, 1)
    gate_part = jnp.dot(gathered, gate_weight, preferred_element_type=jnp.float32)
    up_part = jnp.dot(gathered, up_weight, preferred_element_type=jnp.float32)
    gate_sum, up_sum = in_one_piece((gate_part, up_part), KV, 1, 0)
    hidden_share = (jax.nn.silu(gate_sum) * up_sum).astype(jnp.bfloat16)
    hidden = collect(hidden_share, KV, 1)
    down_part = jnp.dot(hidden, down_weight, preferred_element_type=jnp.float32)
    mixer_out = summed_on_arrival(down_part.astype(jnp.bfloat16), TP, 1)
    return (after_f + mixer_out).astype(jnp.bfloat16)


def solution(mesh):
    split = Mesh(mesh.devices.reshape(4, 4, 4, 2), ("kv_0", "kv_1", "tp_0", "tp_1"))
    placed = (
        P(None, KV_TP),
        P(KV),
        P(KV, TP),
        P(None, KV, TP, None),
        P(None, KV, TP, None),
        P(TP),
        P(),
        P(TP, KV),
        P(KV_TP),
        P(KV, TP),
        P(KV, TP),
        P(TP, KV),
    )
    return jax.shard_map(
        per_device, mesh=split, in_specs=placed, out_specs=P(None, KV_TP), check_vma=False
    )
```

profile of v0, /device:TPU:1, one launch (start us, length us, event | category | flops | bytes accessed | tf_op | source)
XLA Modules:
  0.0 142.8 jit_solution(11357041819467350813)
XLA Ops:
  0.0 0.0 copy-start
  0.0 0.8 broadcast_in_dim.12
  0.8 0.1 reshape.255
  0.9 10.2 %all_to_all.59 = bf16[8,2,256]{2,1,0:T(2,128)(2,1)S(1)} all-to-all(bf16[8,2,256]{2,1,0:T(2,128)(2,1)S(1)} %reshape.255), channel_id=1, replica_groups=mesh['kv_0'=4,'kv_1'=4,'tp_0'=4,'tp_1'=2] {'tp_0','tp_1'}, dimensions={0} | all-to-all | bytes 16384 | tf_op jit(solution)/shard_map/all_to_all | solution.py:22
  11.1 0.1 reshape.256
  11.2 0.1 fusion.14
  11.3 0.1 reshape.253
  11.4 1.1 convolution_bitcast_fusion
  12.5 1.1 broadcast_in_dim.13
  13.6 7.8 %all-to-all-start.1 = ((f32[16,1,8208]{2,1,0:T(1,128)}), f32[16,1,8208]{2,1,0:T(1,128)S(1)}, u32[]{:S(2)}, u32[]{:S(2)}) async-start(f32[16,1,8208]{2,1,0:T(1,128)} %broadcast_in_dim.13), calls=%async_computation.1 | async-start | bytes 1064960 | tf_op jit(solution)/shard_map/all_to_all | solution.py:22
  21.4 6.4 %copy.135 = bf16[16,1024,1,128]{1,3,0,2:T(8,128)(2,1)} copy(bf16[16,1024,1,128]{3,1,2,0:T(8,128)(2,1)} %param.15) | data formatting | bytes 8388608 | tf_op args[3]
  27.8 4.1 %all-to-all-done.1 = f32[16,1,8208]{2,1,0:T(1,128)S(1)} async-done(((f32[16,1,8208]{2,1,0:T(1,128)}), f32[16,1,8208]{2,1,0:T(1,128)S(1)}, u32[]{:S(2)}, u32[]{:S(2)}) %all-to-all-start.1) | async-done | bytes 525344 | tf_op jit(solution)/shard_map/all_to_all | solution.py:22
  31.9 0.3 reduce_sum.93
  32.2 0.1 reshape.242
  32.3 0.1 fusion.18
  32.4 2.9 %fusion.36 = (f32[2,16,4]{2,1,0:T(8,128)S(1)}, f32[2,16,4,1024]{3,2,1,0:T(4,128)S(1)}) fusion(bf16[16,1024,2,64]{1,3,2,0:T(8,128)(2,1)} %bitcast.99, bf16[16,4,2,64]{3,0,2,1:T(8,128)(2,1)S(1)} %fusion.18), kind=kOutput, calls=%fused_computation.65 | convolution fusion | flops 17039232 | bytes 4735488 | tf_op jit(solution)/shard_map/bkgcd,bpkcd->cbkgp/dot_general | solution.py:126
  35.4 0.4 fusion.12
  35.7 0.3 copy.142
  36.0 0.3 copy.141
  36.4 3.0 %fusion.7 = f32[1,2,16,1,4,128]{5,4,1,2,3,0:T(4,128)S(1)} fusion(bf16[16,1024,1,128]{3,1,2,0:T(8,128)(2,1)} %param.16, bf16[2,16,4,1024]{3,2,1,0:T(4,128)(2,1)S(1)} %get-tuple-element.8), kind=kOutput, calls=%fused_computation.5 | convolution fusion | flops 33554432 | bytes 4521984 | tf_op jit(solution)/shard_map/cbkgp,bpkv->cbkgv/dot_general | solution.py:133
  39.3 0.2 maximum_bitcast_fusion
  39.5 10.1 %all_to_all.60 = f32[1,2,16,1,4,130]{5,4,1,3,0,2:T(4,128)S(1)} all-to-all(f32[1,2,16,1,4,130]{5,4,1,3,0,2:T(4,128)S(1)} %maximum_bitcast_fusion), channel_id=1, replica_groups=mesh['kv_0'=4,'kv_1'=4,'tp_0'=4,'tp_1'=2] {'kv_0','kv_1'}, dimensions={2} | all-to-all | bytes 133120 | tf_op jit(solution)/shard_map/all_to_all | solution.py:56
  49.7 0.4 copy.144
  50.1 0.1 slice_reduce_fusion
  50.1 0.1 exponential_bitcast_fusion
  50.2 0.2 fusion.29
  50.4 0.4 fusion.10
  50.8 0.1 copy.146
  50.9 0.0 copy-done.5
  50.9 0.1 copy.147
  51.0 0.1 mul.164
  51.1 0.1 mul.158
  51.1 0.0 copy-done.6
  51.2 0.5 broadcast.113
  51.7 0.7 reduce.12
  52.5 9.5 %all_to_all.61 = bf16[16,2,256]{2,1,0:T(2,128)(2,1)S(1)} all-to-all(bf16[16,2,256]{2,1,0:T(2,128)(2,1)S(1)} %reshape.257), channel_id=1, replica_groups=mesh['kv_0'=4,'kv_1'=4,'tp_0'=4,'tp_1'=2] {'kv_0','kv_1'}, dimensions={0} | all-to-all | bytes 32768 | tf_op jit(solution)/shard_map/all_to_all | solution.py:22
  62.0 0.1 convolution_convert_fusion.1
  62.2 0.1 reshape.248
  62.3 0.1 reshape.259
  62.4 11.0 %all_to_all.62 = bf16[8,2,256]{2,1,0:T(2,128)(2,1)S(1)} all-to-all(bf16[8,2,256]{2,1,0:T(2,128)(2,1)S(1)} %reshape.259), channel_id=1, replica_groups=mesh['kv_0'=4,'kv_1'=4,'tp_0'=4,'tp_1'=2] {'tp_0','tp_1'}, dimensions={0} | all-to-all | bytes 16384 | tf_op jit(solution)/shard_map/all_to_all | solution.py:68
  73.4 0.1 reshape.260
  73.5 0.1 fusion.22
  73.6 6.9 %psum.28 = f32[16]{0:T(128)S(1)} all-reduce(f32[16]{0:T(128)S(1)} %get-tuple-element.5), channel_id=1, replica_groups=mesh['kv_0'=4,'kv_1'=4,'tp_0'=4,'tp_1'=2] {'kv_0'}, use_global_device_ids=true, to_apply=%region_10.0 | all-reduce | flops 16 | bytes 128 | tf_op jit(solution)/shard_map/psum | solution.py:73
  80.5 6.9 %psum.29 = f32[16]{0:T(128)S(1)} all-reduce(f32[16]{0:T(128)S(1)} %psum.28), channel_id=1, replica_groups=mesh['kv_0'=4,'kv_1'=4,'tp_0'=4,'tp_1'=2] {'kv_1'}, use_global_device_ids=true, to_apply=%region_11.0 | all-reduce | flops 16 | bytes 128 | tf_op jit(solution)/shard_map/psum | solution.py:73
  87.4 6.9 %psum.30 = f32[16]{0:T(128)S(1)} all-reduce(f32[16]{0:T(128)S(1)} %psum.29), channel_id=1, replica_groups=mesh['kv_0'=4,'kv_1'=4,'tp_0'=4,'tp_1'=2] {'tp_0'}, use_global_device_ids=true, to_apply=%region_12.0 | all-reduce | flops 16 | bytes 128 | tf_op jit(solution)/shard_map/psum | solution.py:73
  94.3 8.9 %psum.31 = f32[16]{0:T(128)S(1)} all-reduce(f32[16]{0:T(128)S(1)} %psum.30), channel_id=1, replica_groups=mesh['kv_0'=4,'kv_1'=4,'tp_0'=4,'tp_1'=2] {'tp_1'}, use_global_device_ids=true, to_apply=%region_13.0 | all-reduce | flops 16 | bytes 128 | tf_op jit(solution)/shard_map/psum | solution.py:73
  103.1 0.1 fusion.24
  103.2 0.1 reshape.261
  103.3 7.3 %all_to_all.63 = bf16[8,2,256]{2,1,0:T(2,128)(2,1)S(1)} all-to-all(bf16[8,2,256]{2,1,0:T(2,128)(2,1)S(1)} %reshape.261), channel_id=1, replica_groups=mesh['kv_0'=4,'kv_1'=4,'tp_0'=4,'tp_1'=2] {'tp_0','tp_1'}, dimensions={0} | all-to-all | bytes 16384 | tf_op jit(solution)/shard_map/all_to_all | solution.py:22
  110.6 0.1 reshape.262
  110.7 0.1 reshape.249
  110.8 0.2 fusion.37
  111.0 0.2 fusion.38
  111.3 0.2 reshape.250
  111.5 0.1 copy.187
  111.6 10.7 %all_to_all.64 = f32[16,32,88]{2,1,0:T(8,128)S(1)} all-to-all(f32[16,32,88]{2,1,0:T(8,128)S(1)} %bitcast.104), channel_id=1, replica_groups=mesh['kv_0'=4,'kv_1'=4,'tp_0'=4,'tp_1'=2] {'kv_0','kv_1'}, dimensions={0} | all-to-all | bytes 360448 | tf_op jit(solution)/shard_map/all_to_all | solution.py:78
  122.4 9.1 %all_to_all.65 = bf16[16,16,88]{2,1,0:T(8,128)(2,1)S(1)} all-to-all(bf16[16,16,88]{2,1,0:T(8,128)(2,1)S(1)} %broadcast_in_dim.17), channel_id=1, replica_groups=mesh['kv_0'=4,'kv_1'=4,'tp_0'=4,'tp_1'=2] {'kv_0','kv_1'}, dimensions={0} | all-to-all | bytes 90112 | tf_op jit(solution)/shard_map/all_to_all | solution.py:22
  131.5 0.1 reshape.251
  131.7 0.2 convolution_convert_fusion
  131.9 0.1 reshape.252
  132.0 0.1 reshape.263
  132.1 10.0 %all_to_all.66 = bf16[8,2,256]{2,1,0:T(2,128)(2,1)S(1)} all-to-all(bf16[8,2,256]{2,1,0:T(2,128)(2,1)S(1)} %reshape.263), channel_id=1, replica_groups=mesh['kv_0'=4,'kv_1'=4,'tp_0'=4,'tp_1'=2] {'tp_0','tp_1'}, dimensions={0} | all-to-all | bytes 16384 | tf_op jit(solution)/shard_map/all_to_all | solution.py:68
  142.1 0.1 reshape.264
  142.2 0.6 fusion.25
  (41 shorter events, 0.4 us)
Async XLA Ops:
  0.0 110.8 %copy-start = (bf16[256,1408]{1,0:T(8,128)(2,1)S(1)}, bf16[256,1408]{1,0:T(8,128)(2,1)}, u32[]{:S(2)}) copy-start(bf16[256,1408]{1,0:T(8,128)(2,1)} %param.21) | copy-start | bytes 2162692
  13.6 18.3 %all-to-all-start.1 = ((f32[16,1,8208]{2,1,0:T(1,128)}), f32[16,1,8208]{2,1,0:T(1,128)S(1)}, u32[]{:S(2)}, u32[]{:S(2)}) async-start(f32[16,1,8208]{2,1,0:T(1,128)} %broadcast_in_dim.13), calls=%async_computation.1 | async-start | bytes 1064960 | tf_op jit(solution)/shard_map/all_to_all | solution.py:22
  35.3 15.5 %copy-start.5 = (f32[4]{0:T(128)S(1)}, f32[4]{0:T(128)}, u32[]{:S(2)}) copy-start(f32[4]{0:T(128)} %param.17) | copy-start | bytes 52
  35.4 15.8 %copy-start.6 = (f32[128]{0:T(128)S(1)}, f32[128]{0:T(128)}, u32[]{:S(2)}) copy-start(f32[128]{0:T(128)} %param.18) | copy-start | bytes 1540
  35.4 26.7 %copy-start.3 = (bf16[512,256]{1,0:T(8,128)(2,1)S(1)}, bf16[512,256]{1,0:T(8,128)(2,1)}, u32[]{:S(2)}) copy-start(bf16[512,256]{1,0:T(8,128)(2,1)} %param.19) | copy-start | bytes 786436
  36.0 37.5 %copy-start.4 = (bf16[16,32]{1,0:T(8,128)(2,1)S(1)}, bf16[16,32]{1,0:T(8,128)(2,1)}, u32[]{:S(2)}) copy-start(bf16[16,32]{1,0:T(8,128)(2,1)} %param.12) | copy-start | bytes 3076
  36.0 67.1 %copy-start.7 = (f32[32]{0:T(128)S(1)}, f32[32]{0:T(128)}, u32[]{:S(2)}) copy-start(f32[32]{0:T(128)} %param.20) | copy-start | bytes 388
  36.3 74.7 %copy-start.1 = (bf16[256,1408]{1,0:T(8,128)(2,1)S(1)}, bf16[256,1408]{1,0:T(8,128)(2,1)}, u32[]{:S(2)}) copy-start(bf16[256,1408]{1,0:T(8,128)(2,1)} %param.22) | copy-start | bytes 2162692
  39.3 92.3 %copy-start.2 = (bf16[1408,256]{1,0:T(8,128)(2,1)S(1)}, bf16[1408,256]{1,0:T(8,128)(2,1)}, u32[]{:S(2)}) copy-start(bf16[1408,256]{1,0:T(8,128)(2,1)} %param.23) | copy-start | bytes 2162692
where the time goes:
time: 144 us; the launch traced here: 143 us
  blocking collectives  107 us (74%)
  local copies, waits for them, and re-layouts  11.9 us (8%)
  matrix products  7.77 us (5%)
  starting transfers between devices  7.77 us (5%)
  waiting for transfers between devices  4.08 us (3%)
  other arithmetic  3.54 us (2%)
    all_to_all x4, blocking collectives, from_everyone(): lax.all_to_all(jnp.broadcast_to(shard[None], (length, *shard.shape)), axi...  36.2 us
    psum x4, blocking collectives, by_axis(): return functools.reduce(lax.psum, axes, shard)  29.5 us
    all_to_all x2, blocking collectives, summed_on_arrival(): lax.all_to_all(tiles, axis, split_axis=0, concat_axis=0, tiled=True)  21 us
    all_to_all x1, blocking collectives, sent_and_summed(): lax.all_to_all(cut_along(shard, dim, length), axis, 0, 0, tiled=True)  10.7 us
    all_to_all x1, blocking collectives, side_by_side(): lax.all_to_all(both, axis, split_axis=split_dim, concat_axis=concat_dim,...  10.1 us
    all_to_all x1, starting transfers between devices, from_everyone(): lax.all_to_all(jnp.broadcast_to(shard[None], (length, *shard.shape)), axi...  7.77 us
    unnamed x28, local copies, waits for them, and re-layouts  7.24 us
    all_to_all x1, waiting for transfers between devices, from_everyone(): lax.all_to_all(jnp.broadcast_to(shard[None], (length, *shard.shape)), axi...  4.08 us
  transfers between devices with their start and end apart: 1, of which 1 were waited for; matrix products, arithmetic and copies ran while one was open for 4% of the time, Pallas kernels for 0%

commit v1 on v0

v1 whole, which is shorter than its diff:
```python
import functools

import jax
import jax.numpy as jnp
from jax import lax
from jax.experimental import pallas as pl
from jax.experimental.pallas import tpu as pltpu
from jax.sharding import PartitionSpec as P

MESH = pl.DeviceIdType.MESH
F32, BF16 = jnp.float32, jnp.bfloat16

D = 4096
HEAD_DIM = 64
EPS = 1e-06

KV_OFFSETS = sorted(range(1, 16), key=lambda d: -(min(d // 4, 4 - d // 4) + min(d % 4, 4 - d % 4)))
TP_OFFSETS = sorted(range(1, 8), key=lambda d: -min(d // 2, 4 - d // 2))


def kernel(
    hid_hbm, ag_hbm, wq_hbm, k_hbm, v_hbm, lam_hbm, hg_hbm, wo_hbm, mg_hbm, wg_hbm, wu_hbm, wd_hbm,
    out_ref,
    hid, ag, wq, kc, vc, lam, hg, wo, mg, wg, wu, wd,
    g1, g1m, s2, r2, a3, s4, r4, a5, f5, a6, s7, r7, a8, f8, s9, r9,
    load_sem, send_sem, recv_sem,
):
    kv, tp = lax.axis_index("kv"), lax.axis_index("tp")
    z, y, x, core = kv // 4, kv % 4, tp // 2, tp % 2

    def kv_peer(d):
        return ((z + d // 4) % 4) * 4 + (y + d % 4) % 4

    def tp_peer(d):
        return ((x + d // 2) % 4) * 2 + (core + d % 2) % 2

    loads = [
        pltpu.make_async_copy(src, dst, load_sem.at[n])
        for n, (src, dst) in enumerate([
            (hid_hbm, hid), (mg_hbm, mg), (ag_hbm, ag), (wq_hbm, wq), (k_hbm, kc), (v_hbm, vc),
            (lam_hbm, lam), (hg_hbm, hg), (wo_hbm, wo), (wg_hbm, wg), (wu_hbm, wu), (wd_hbm, wd),
        ])
    ]
    L_HID, L_MG, L_AG, L_WQ, L_K, L_V, L_LAM, L_HG, L_WO, L_WG, L_WU, L_WD = loads
    for load in loads:
        load.start()

    barrier = pltpu.get_barrier_semaphore()
    for d in KV_OFFSETS:
        pl.semaphore_signal(barrier, inc=1, device_id={"kv": kv_peer(d), "tp": tp}, device_id_type=MESH)
    for d in TP_OFFSETS:
        pl.semaphore_signal(barrier, inc=1, device_id={"kv": kv, "tp": tp_peer(d)}, device_id_type=MESH)

    def to_kv(phase, src, dst):
        for d in KV_OFFSETS:
            peer = kv_peer(d)
            pltpu.make_async_remote_copy(
                src(peer, d), dst(peer, d), send_sem.at[phase], recv_sem.at[phase],
                device_id={"kv": peer, "tp": tp}, device_id_type=MESH,
            ).start()

    def to_tp(phase, src, dst):
        for d in TP_OFFSETS:
            peer = tp_peer(d)
            pltpu.make_async_remote_copy(
                src(peer, d), dst(peer, d), send_sem.at[phase], recv_sem.at[phase],
                device_id={"kv": kv, "tp": peer}, device_id_type=MESH,
            ).start()

    def wait_bytes(ref, sem):
        pltpu.make_async_copy(ref, ref, sem).wait()

    L_HID.wait()
    L_MG.wait()
    lane = lax.broadcasted_iota(jnp.int32, (16, 128), 1)
    mine = lane // 32 == tp % 4
    h32 = hid[...].astype(F32)
    g1[tp] = jnp.where(mine, jnp.concatenate([h32] * 4, axis=1), 0.0).astype(BF16)
    g1m[tp] = jnp.where(mine[0:1], jnp.concatenate([mg[...]] * 4, axis=1), 0.0)

    pl.semaphore_wait(barrier, 22)

    to_tp(0, lambda peer, d: g1.at[tp], lambda peer, d: g1.at[tp])
    to_tp(9, lambda peer, d: g1m.at[tp], lambda peer, d: g1m.at[tp])
    L_AG.wait()
    L_WQ.wait()
    wait_bytes(g1.at[pl.ds(0, 7)], recv_sem.at[0])
    hid_f = jnp.concatenate([sum(g1[n].astype(F32) for n in range(h, h + 4)) for h in (0, 4)], axis=1)
    squares = jnp.sum(hid_f * hid_f, axis=1, keepdims=True)
    gained = (hid_f * ag[...]).astype(BF16)
    partial = jnp.dot(gained, wq[...], preferred_element_type=F32)
    for c in range(4):
        s2[pl.ds(c, 16, stride=8), :] = partial[:, 128 * c : 128 * (c + 1)]
    s2[pl.ds(4, 16, stride=8), :] = jnp.broadcast_to(squares, (16, 128))

    to_kv(1, lambda peer, d: s2.at[pl.ds(pl.multiple_of(peer * 8, 8), 8)], lambda peer, d: r2.at[pl.ds(8 * d, 8)])
    own = s2[pl.ds(pl.multiple_of(kv * 8, 8), 8), :]
    wait_bytes(r2.at[pl.ds(0, 120)], recv_sem.at[1])
    tot = own + sum(r2[8 * d : 8 * d + 8, :] for d in range(1, 16))
    inv = lax.rsqrt(tot[4:5] / D + EPS)
    q4 = (tot[0:4] * inv).astype(BF16).astype(F32)
    low = lane[0:4] < HEAD_DIM
    a3[kv] = jnp.concatenate([jnp.where(low, q4, 0.0), jnp.where(low, 0.0, q4)], axis=0).astype(BF16)

    to_kv(2, lambda peer, d: a3.at[kv], lambda peer, d: a3.at[kv])
    L_K.wait()
    L_V.wait()
    wait_bytes(a3.at[pl.ds(0, 15)], recv_sem.at[2])

    upper = lax.broadcasted_iota(jnp.int32, (16, 128), 0) < 8

    def pair(p, _):
        both = jnp.concatenate([a3[2 * p].astype(F32), a3[2 * p + 1].astype(F32)], axis=0)
        lhs = jnp.concatenate([jnp.where(upper, both, 0.0), jnp.where(upper, 0.0, both)], axis=1).astype(BF16)
        keys = jnp.concatenate([kc[2 * p], kc[2 * p + 1]], axis=1)
        scores = lax.dot_general(lhs, keys, (((1,), (1,)), ((), ())), preferred_element_type=F32) * HEAD_DIM**-0.5
        top = jnp.max(scores, axis=1, keepdims=True)
        exponent = jnp.exp(scores - top)
        total = jnp.sum(exponent, axis=1, keepdims=True)
        values = jnp.concatenate([vc[2 * p], vc[2 * p + 1]], axis=1)
        acc = jnp.dot(exponent.astype(BF16), values, preferred_element_type=F32)
        stats = jnp.where(lane < 64, top, total)
        row = pl.multiple_of(p * 32, 32)
        s4[pl.ds(row, 8), :] = acc[0:8, 0:128]
        s4[pl.ds(row + 8, 8), :] = stats[0:8]
        s4[pl.ds(row + 16, 8), :] = acc[8:16, 128:256]
        s4[pl.ds(row + 24, 8), :] = stats[8:16]
        return 0

    lax.fori_loop(0, 8, pair, 0)

    to_kv(3, lambda peer, d: s4.at[pl.ds(pl.multiple_of(peer * 16, 16), 16)], lambda peer, d: r4.at[pl.ds(16 * d, 16)])
    L_LAM.wait()
    L_HG.wait()
    row8 = lax.broadcasted_iota(jnp.int32, (8, 128), 0)
    lane8 = lane[0:8]
    mixing = jnp.sum(jnp.where(row8 == lane8, jnp.concatenate([lam[...], jnp.zeros((1, 124), F32)], axis=1), 0.0), axis=1, keepdims=True)
    own_acc = s4[pl.ds(pl.multiple_of(kv * 16, 16), 8), :]
    own_stats = s4[pl.ds(pl.multiple_of(kv * 16 + 8, 8), 8), :]
    wait_bytes(r4.at[pl.ds(0, 240)], recv_sem.at[3])
    accs = [own_acc] + [r4[16 * d : 16 * d + 8, :] for d in range(1, 16)]
    stats = [own_stats] + [r4[16 * d + 8 : 16 * d + 16, :] for d in range(1, 16)]
    top = functools.reduce(jnp.maximum, stats)
    own_tot, own_sum = 0.0, 0.0
    for a, s in zip(accs, stats):
        factor = jnp.exp(jnp.where(lane8 < 64, s - top, 0.0))
        factor = jnp.where(lane8 < 64, factor, pltpu.roll(factor, 64, axis=1))
        own_sum += a * factor
        own_tot += s * factor
    own_tot = jnp.where(lane8 < 64, pltpu.roll(own_tot, 64, axis=1), own_tot)
    means = own_sum / own_tot
    attended = means - mixing * pltpu.roll(means, 4, axis=0)
    norm_inv = lax.rsqrt(jnp.mean(attended * attended, axis=1, keepdims=True) + EPS)
    a5[kv] = (attended * norm_inv * hg[...]).astype(BF16)

    to_kv(4, lambda peer, d: a5.at[kv], lambda peer, d: a5.at[kv])
    L_WO.wait()
    wait_bytes(a5.at[pl.ds(0, 15)], recv_sem.at[4])
    for b in range(16):
        f5[8 * b : 8 * b + 8, :] = a5[b].astype(F32)
    head_out = jnp.concatenate([f5[pl.ds(c, 16, stride=8), :] for c in range(4)], axis=1).astype(BF16)
    a6[tp] = jnp.dot(head_out, wo[...], preferred_element_type=F32).astype(BF16)

    to_tp(5, lambda peer, d: a6.at[tp], lambda peer, d: a6.at[tp])
    wait_bytes(g1m.at[pl.ds(0, 7)], recv_sem.at[9])
    gain2 = jnp.concatenate([sum(g1m[n] for n in range(h, h + 4)) for h in (0, 4)], axis=1)
    L_WG.wait()
    L_WU.wait()
    wait_bytes(a6.at[pl.ds(0, 7)], recv_sem.at[5])
    after_f = (hid_f + sum(a6[n].astype(F32) for n in range(8))).astype(BF16).astype(F32)
    squares2 = jnp.sum(after_f * after_f, axis=1, keepdims=True)
    gained2 = (after_f * gain2).astype(BF16)
    gate = jnp.dot(gained2, wg[...], preferred_element_type=F32)
    for c in range(11):
        s7[pl.ds(c, 16, stride=24), :] = gate[:, 128 * c : 128 * (c + 1)]
    up = jnp.dot(gained2, wu[...], preferred_element_type=F32)
    for c in range(11):
        s7[pl.ds(11 + c, 16, stride=24), :] = up[:, 128 * c : 128 * (c + 1)]
    s7[pl.ds(22, 16, stride=24), :] = jnp.broadcast_to(squares2, (16, 128))

    to_kv(6, lambda peer, d: s7.at[pl.ds(pl.multiple_of(peer * 24, 8), 24)], lambda peer, d: r7.at[pl.ds(24 * d, 24)])
    own = s7[pl.ds(pl.multiple_of(kv * 24, 8), 24), :]
    wait_bytes(r7.at[pl.ds(0, 360)], recv_sem.at[6])
    tot = own + sum(r7[24 * d : 24 * d + 24, :] for d in range(1, 16))
    inv2 = lax.rsqrt(tot[22:23] / D + EPS)
    tot = tot * inv2
    gate_sum, up_sum = tot[0:16], jnp.concatenate([tot[11:22], tot[0:5]], axis=0)
    a8[kv] = (gate_sum / (1.0 + jnp.exp(-gate_sum)) * up_sum).astype(BF16)

    to_kv(7, lambda peer, d: a8.at[kv], lambda peer, d: a8.at[kv])
    L_WD.wait()
    wait_bytes(a8.at[pl.ds(0, 15)], recv_sem.at[7])
    for b in range(16):
        f8[16 * b : 16 * b + 16, :] = a8[b].astype(F32)
    hidden = jnp.concatenate([f8[pl.ds(c, 16, stride=16), :] for c in range(11)], axis=1).astype(BF16)
    down = jnp.dot(hidden, wd[...], preferred_element_type=F32).astype(BF16)
    s9[0] = down[:, 0:128]
    s9[1] = down[:, 128:256]

    to_tp(8, lambda peer, d: s9.at[peer // 4], lambda peer, d: r9.at[d])
    own = s9[tp // 4].astype(F32)
    after_own = jnp.where(tp // 4 == 0, after_f[:, 0:128], after_f[:, 128:256])
    wait_bytes(r9.at[pl.ds(0, 7)], recv_sem.at[8])
    mixed = after_own + (own + sum(r9[d].astype(F32) for d in range(1, 8)))
    out_ref[...] = pltpu.roll(mixed, (4 - tp % 4) % 4 * 32, axis=1)[:, 0:32].astype(BF16)

    for phase, ref in enumerate([
        g1.at[pl.ds(0, 7)], r2.at[pl.ds(0, 120)], a3.at[pl.ds(0, 15)], r4.at[pl.ds(0, 240)], a5.at[pl.ds(0, 15)],
        a6.at[pl.ds(0, 7)], r7.at[pl.ds(0, 360)], a8.at[pl.ds(0, 15)], r9.at[pl.ds(0, 7)], g1m.at[pl.ds(0, 7)],
    ]):
        wait_bytes(ref, send_sem.at[phase])


def per_device(hidden_in, attn_gain, query_weight, key_cache, value_cache, lambdas, head_gain, out_weight,
               mixer_gain, gate_weight, up_weight, down_weight):
    args = (
        hidden_in, attn_gain.reshape(1, 256), query_weight, key_cache.reshape(16, 1024, 128), value_cache.reshape(16, 1024, 128),
        lambdas.reshape(1, 4), head_gain.reshape(1, 128), out_weight, mixer_gain.reshape(1, 32), gate_weight, up_weight, down_weight,
    )
    V = pltpu.VMEM
    return pl.pallas_call(
        kernel,
        name="layer",
        out_shape=jax.ShapeDtypeStruct((16, 32), BF16),
        in_specs=[pl.BlockSpec(memory_space=pl.ANY)] * len(args),
        out_specs=pl.BlockSpec(memory_space=pltpu.VMEM),
        scratch_shapes=[
            *(V(a.shape, a.dtype) for a in args),
            V((8, 16, 128), BF16), V((8, 1, 128), F32),
            V((128, 128), F32), V((128, 128), F32), V((16, 8, 128), BF16),
            V((256, 128), F32), V((256, 128), F32), V((16, 8, 128), BF16), V((128, 128), F32),
            V((8, 16, 256), BF16),
            V((384, 128), F32), V((384, 128), F32), V((16, 16, 128), BF16), V((256, 128), F32),
            V((2, 16, 128), BF16), V((8, 16, 128), BF16),
            pltpu.SemaphoreType.DMA((12,)), pltpu.SemaphoreType.DMA((10,)), pltpu.SemaphoreType.DMA((10,)),
        ],
        compiler_params=pltpu.CompilerParams(collective_id=0, has_side_effects=True, vmem_limit_bytes=48 * 2**20),
    )(*args)


def solution(mesh):
    placed = (
        P(None, ("kv", "tp")), P("kv"), P("kv", "tp"), P(None, "kv", "tp", None), P(None, "kv", "tp", None), P("tp"),
        P(), P("tp", "kv"), P(("kv", "tp")), P("kv", "tp"), P("kv", "tp"), P("tp", "kv"),
    )
    return jax.shard_map(per_device, mesh=mesh, in_specs=placed, out_specs=P(None, ("kv", "tp")), check_vma=False)
```

time: 144 us -> 64.5 us (0.45)
  blocking collectives: 107 us -> 0 us
  Pallas kernels: 0 us -> 55 us
  matrix products: 7.77 us -> 0 us
  starting transfers between devices: 7.77 us -> 0 us
  waiting for transfers between devices: 4.08 us -> 0 us
  other arithmetic: 3.54 us -> 0 us
  local copies, waits for them, and re-layouts: 11.9 us -> 9.15 us
    all_to_all x8 -> x0, blocking collectives: 77.9 us -> none  [the longest x4 36.2 us: from_everyone(): lax.all_to_all(jnp.broadcast_to(shard[None], (length, *shard.shape)), axi...]
    pallas_call x0 -> x1, Pallas kernels: none -> 55 us  [per_device(): pl.pallas_call(kernel, name='layer', out_shape=jax.ShapeDtypeStruct((16,...]
    psum x4 -> x0, blocking collectives: 29.5 us -> none  [by_axis(): return functools.reduce(lax.psum, axes, shard)]
    dot_general x7 -> x0, matrix products: 7.77 us -> none  [the longest x1 2.98 us: per_device(): jnp.einsum('cbkgp,bpkv->cbkgv', exp_weights, value_cache, preferred_eleme...]
    all_to_all x1 -> x0, starting transfers between devices: 7.77 us -> none  [from_everyone(): lax.all_to_all(jnp.broadcast_to(shard[None], (length, *shard.shape)), axi...]
    all_to_all x1 -> x0, waiting for transfers between devices: 4.08 us -> none  [from_everyone(): lax.all_to_all(jnp.broadcast_to(shard[None], (length, *shard.shape)), axi...]
    broadcast_in_dim x6 -> x0, local copies, waits for them, and re-layouts: 2.38 us -> none  [from_everyone(): jnp.broadcast_to(shard[None], (length, *shard.shape))]
    unnamed x28 -> x21, local copies, waits for them, and re-layouts: 7.24 us -> 9.15 us
  transfers between devices with their start and end apart: 1 -> 0, of which waited for: 1 -> 0; matrix products, arithmetic and copies ran while one was open for 4% -> 0% of each run, Pallas kernels for 0% -> 0%
where the time goes in v1:
time: 64.5 us; the launch traced here: 64.2 us
  Pallas kernels  55 us (85%)
  local copies, waits for them, and re-layouts  9.15 us (14%)
    pallas_call x1, Pallas kernels, per_device(): pl.pallas_call(kernel, name='layer', out_shape=jax.ShapeDtypeStruct((16,...  55 us
    unnamed x21, local copies, waits for them, and re-layouts  9.15 us

profile of v1, /device:TPU:1, one launch (start us, length us, event | category | flops | bytes accessed | tf_op | source)
XLA Modules:
  0.0 64.2 jit_solution(16861098859919872388)
XLA Ops:
  0.0 0.0 copy-start
  0.0 1.1 %copy-done = bf16[256,1408]{1,0:T(8,128)(2,1)S(1)} copy-done((bf16[256,1408]{1,0:T(8,128)(2,1)S(1)}, bf16[256,1408]{1,0:T(8,128)(2,1)}, u32[]{:S(2)}) %copy-start) | copy-done | bytes 720920
  1.1 0.0 copy-start.1
  1.1 1.1 %copy-done.1 = bf16[256,1408]{1,0:T(8,128)(2,1)S(1)} copy-done((bf16[256,1408]{1,0:T(8,128)(2,1)S(1)}, bf16[256,1408]{1,0:T(8,128)(2,1)}, u32[]{:S(2)}) %copy-start.1) | copy-done | bytes 720920
  2.2 0.0 copy-start.2
  2.2 1.1 %copy-done.2 = bf16[1408,256]{1,0:T(8,128)(2,1)S(1)} copy-done((bf16[1408,256]{1,0:T(8,128)(2,1)S(1)}, bf16[1408,256]{1,0:T(8,128)(2,1)}, u32[]{:S(2)}) %copy-start.2) | copy-done | bytes 720920
  3.3 0.0 copy-start.3
  3.3 0.9 %copy-done.3 = bf16[256,512]{1,0:T(8,128)(2,1)S(1)} copy-done((bf16[256,512]{1,0:T(8,128)(2,1)S(1)}, bf16[256,512]{1,0:T(8,128)(2,1)}, u32[]{:S(2)}) %copy-start.3) | copy-done | bytes 262168
  4.3 0.0 copy-start.4
  4.3 0.9 %copy-done.4 = bf16[512,256]{1,0:T(8,128)(2,1)S(1)} copy-done((bf16[512,256]{1,0:T(8,128)(2,1)S(1)}, bf16[512,256]{1,0:T(8,128)(2,1)}, u32[]{:S(2)}) %copy-start.4) | copy-done | bytes 262168
  5.2 0.0 copy-start.5
  5.2 0.7 %copy-done.5 = bf16[16,32]{1,0:T(8,128)(2,1)S(1)} copy-done((bf16[16,32]{1,0:T(8,128)(2,1)S(1)}, bf16[16,32]{1,0:T(8,128)(2,1)}, u32[]{:S(2)}) %copy-start.5) | copy-done | bytes 1048
  5.9 0.0 copy-start.6
  5.9 0.7 %copy-done.6 = f32[256]{0:T(256)S(1)} copy-done((f32[256]{0:T(256)S(1)}, f32[256]{0:T(256)}, u32[]{:S(2)}) %copy-start.6) | copy-done | bytes 1048
  6.6 0.0 copy-start.7
  6.6 0.7 %copy-done.7 = f32[4]{0:T(128)S(1)} copy-done((f32[4]{0:T(128)S(1)}, f32[4]{0:T(128)}, u32[]{:S(2)}) %copy-start.7) | copy-done | bytes 40
  7.3 0.0 copy-start.8
  7.3 0.7 %copy-done.8 = f32[128]{0:T(128)S(1)} copy-done((f32[128]{0:T(128)S(1)}, f32[128]{0:T(128)}, u32[]{:S(2)}) %copy-start.8) | copy-done | bytes 536
  7.9 0.0 copy-start.9
  7.9 0.7 %copy-done.9 = f32[32]{0:T(128)S(1)} copy-done((f32[32]{0:T(128)S(1)}, f32[32]{0:T(128)}, u32[]{:S(2)}) %copy-start.9) | copy-done | bytes 152
  8.6 55.0 %layer.1 = bf16[16,32]{1,0:T(8,128)(2,1)S(1)} custom-call(bf16[16,32]{1,0:T(8,128)(2,1)S(1)} %copy-done.5, f32[1,256]{1,0:T(1,128)S(1)} %bitcast.6, bf16[256,512]{1,0:T(8,128)(2,1)S(1)} %copy-done.3, bf16[16,1024,128]{2,1,0:T(8,128)(2,1)} %bitcast.10, bf16[16,1024,128]{2,1,0:T(8,128)(2,1)} %bitcast.11, f32[1,4]{1,0:T(1,128)S(1)} %bitcast.7, ...), custom_call_target="tpu_custom_call" | custom-call | tf_op jit(solution)/shard_map/layer/pallas_call | solution.py:221
  63.6 0.6 copy.14
Async XLA Ops:
  0.0 1.1 %copy-start = (bf16[256,1408]{1,0:T(8,128)(2,1)S(1)}, bf16[256,1408]{1,0:T(8,128)(2,1)}, u32[]{:S(2)}) copy-start(bf16[256,1408]{1,0:T(8,128)(2,1)} %wg_hbm.1) | copy-start | bytes 2162692
  1.1 1.1 %copy-start.1 = (bf16[256,1408]{1,0:T(8,128)(2,1)S(1)}, bf16[256,1408]{1,0:T(8,128)(2,1)}, u32[]{:S(2)}) copy-start(bf16[256,1408]{1,0:T(8,128)(2,1)} %wu_hbm.1) | copy-start | bytes 2162692
  2.2 1.1 %copy-start.2 = (bf16[1408,256]{1,0:T(8,128)(2,1)S(1)}, bf16[1408,256]{1,0:T(8,128)(2,1)}, u32[]{:S(2)}) copy-start(bf16[1408,256]{1,0:T(8,128)(2,1)} %wd_hbm.1) | copy-start | bytes 2162692
  3.3 0.9 %copy-start.3 = (bf16[256,512]{1,0:T(8,128)(2,1)S(1)}, bf16[256,512]{1,0:T(8,128)(2,1)}, u32[]{:S(2)}) copy-start(bf16[256,512]{1,0:T(8,128)(2,1)} %wq_hbm.1) | copy-start | bytes 786436
  4.3 0.9 %copy-start.4 = (bf16[512,256]{1,0:T(8,128)(2,1)S(1)}, bf16[512,256]{1,0:T(8,128)(2,1)}, u32[]{:S(2)}) copy-start(bf16[512,256]{1,0:T(8,128)(2,1)} %wo_hbm.1) | copy-start | bytes 786436
  5.2 0.7 %copy-start.5 = (bf16[16,32]{1,0:T(8,128)(2,1)S(1)}, bf16[16,32]{1,0:T(8,128)(2,1)}, u32[]{:S(2)}) copy-start(bf16[16,32]{1,0:T(8,128)(2,1)} %hid_hbm.1) | copy-start | bytes 3076
  5.9 0.7 %copy-start.6 = (f32[256]{0:T(256)S(1)}, f32[256]{0:T(256)}, u32[]{:S(2)}) copy-start(f32[256]{0:T(256)} %param.13) | copy-start | bytes 3076
  6.6 0.7 %copy-start.7 = (f32[4]{0:T(128)S(1)}, f32[4]{0:T(128)}, u32[]{:S(2)}) copy-start(f32[4]{0:T(128)} %param.17) | copy-start | bytes 52
  7.3 0.7 %copy-start.8 = (f32[128]{0:T(128)S(1)}, f32[128]{0:T(128)}, u32[]{:S(2)}) copy-start(f32[128]{0:T(128)} %param.18) | copy-start | bytes 1540
  7.9 0.7 %copy-start.9 = (f32[32]{0:T(128)S(1)}, f32[32]{0:T(128)}, u32[]{:S(2)}) copy-start(f32[32]{0:T(128)} %param.20) | copy-start | bytes 388
